TPU v7x, 32 devices: a whole 2x2x4 slice. The times are simulated.
32 devices in a mesh: sp: 8 (over z, y), tp: 4 (over x, core).
Axes of the slice: x: 2, y: 2, z: 4, core: 2. Of those that a mesh axis runs over, the one named last changes fastest.
Arguments:
- tokens: bfloat16 [1536, 2048], P(('sp', 'tp')), may hold values from -6 to 6
- norm_in: float32 [2048], replicated, may hold values from 0.1 to 1.9
- decay_log: float32 [128, 64], P('tp'), may hold values from -0.034 to -0.00016276042, as said below
- phase: float32 [128, 64], P('tp'), may hold values from -1 to 1
- b_real: float32 [128, 64, 16], P('tp'), may hold values from -1 to 1
- b_imag: float32 [128, 64, 16], P('tp'), may hold values from -1 to 1
- c_real: float32 [128, 16, 64], P('tp'), may hold values from -0.75 to 0.75
- c_imag: float32 [128, 16, 64], P('tp'), may hold values from -0.75 to 0.75
- skip_gain: float32 [2048], P('tp'), may hold values from -6 to 6
- w_value: bfloat16 [2048, 2048], P(None, 'tp'), as said below
- w_gate: bfloat16 [2048, 2048], P(None, 'tp'), may hold values from -0.125 to 0.125
- norm_out: float32 [2048], P('tp'), may hold values from 0.1 to 1.9
Outputs:
- mixed: bfloat16 [1536, 2048], P('sp', 'tp')
Inputs may be any that keep to these rules, and one draw needn't show every extreme that they name: `decay_log`: negative real parts of the eigenvalues. `w_value`: weights of the value projection.
All inputs are finite; a program needn't handle non-finite values.
Results may differ from a plain program's by a relative error of at most 0.012.
The roundings to bfloat16 on the way count: a program that leaves them out, or rounds other values in their place, can miss the bound.
Values may be sent and summed in bfloat16 or wider, within the bound.
No kernel may reach another device: no remote copies, remote signals or barrier semaphores. Data moves between devices by JAX's collectives and lax.ppermute only.
A program may use at most 64 MiB of HBM per device.

v0:
```python
import jax
import jax.numpy as jnp
from jax import lax
from jax.sharding import PartitionSpec as P

D = 2048


NORM_EPS = 1e-06
HIGHEST_PREC = lax.Precision.HIGHEST


def entering(value, axis, join, neutral):
    count, mine = (lax.axis_size(axis), lax.axis_index(axis))
    pieces = jax.tree.map(lambda part: lax.all_gather(part, axis), value)
    subtotal = jax.tree.map(
        lambda part, zero: jnp.full_like(part, 0) + jnp.asarray(zero, part.dtype), value, neutral
    )

    def hop(position, subtotal):
        longer = join(subtotal, jax.tree.map(lambda part: part[position], pieces))
        return jax.tree.map(lambda new, old: jnp.where(position < mine, new, old), longer, subtotal)

    return lax.fori_loop(0, count - 1, hop, subtotal)


def coefficients(decay_log, phase, b_real, b_imag):
    magnitude = jnp.exp(decay_log)
    bar_re = magnitude * jnp.cos(phase)
    bar_im = magnitude * jnp.sin(phase)
    modulus = decay_log * decay_log + phase * phase
    coef_re = ((bar_re - 1.0) * decay_log + bar_im * phase) / modulus
    coef_im = (bar_im * decay_log - (bar_re - 1.0) * phase) / modulus
    in_re = coef_re[:, :, None] * b_real - coef_im[:, :, None] * b_imag
    in_im = coef_re[:, :, None] * b_imag + coef_im[:, :, None] * b_real
    return (bar_re, bar_im, in_re, in_im)


def prefix_states(drive_re, drive_im, rate_re, rate_im):
    length = drive_re.shape[0]
    stride = 1
    for level in range(max(length - 1, 1).bit_length()):
        padding = jnp.zeros((stride,) + drive_re.shape[1:], jnp.float32)
        moved_re = jnp.concatenate([padding, drive_re[: length - stride]], axis=0)
        moved_im = jnp.concatenate([padding, drive_im[: length - stride]], axis=0)
        drive_re, drive_im = (
            drive_re + rate_re * moved_re - rate_im * moved_im,
            drive_im + rate_re * moved_im + rate_im * moved_re,
        )
        rate_re, rate_im = (rate_re * rate_re - rate_im * rate_im, 2.0 * rate_re * rate_im)
        stride = stride * 2
    return (drive_re, drive_im)


def readout(state_re, state_im, c_real, c_imag):
    first = jnp.einsum("tgp,ghp->tgh", state_re, c_real, precision=HIGHEST_PREC)
    second = jnp.einsum("tgp,ghp->tgh", state_im, c_imag, precision=HIGHEST_PREC)
    return first - second


def powers(decay_log, phase, exponents):
    magnitude = jnp.exp(exponents[:, None, None] * decay_log[None])
    angles = exponents[:, None, None] * phase[None]
    return (magnitude * jnp.cos(angles), magnitude * jnp.sin(angles))


def combine(earlier, later):
    first_re, first_im, held_re, held_im = earlier
    second_re, second_im, own_re, own_im = later
    return (
        first_re * second_re - first_im * second_im,
        first_re * second_im + first_im * second_re,
        second_re * held_re - second_im * held_im + own_re,
        second_re * held_im + second_im * held_re + own_im,
    )


def on_device(
    tokens,
    norm_in,
    decay_log,
    phase,
    b_real,
    b_imag,
    c_real,
    c_imag,
    skip_gain,
    w_value,
    w_gate,
    norm_out,
):
    xf = tokens.astype(jnp.float32)
    normed = (xf * lax.rsqrt(jnp.mean(xf * xf, axis=1, keepdims=True) + NORM_EPS) * norm_in).astype(
        jnp.bfloat16
    )
    by_channel = lax.all_to_all(normed, "tp", split_axis=1, concat_axis=0, tiled=True)
    row_total, width = by_channel.shape
    groups = decay_log.shape[0]
    drive = by_channel.astype(jnp.float32).reshape(row_total, groups, width // groups)
    bar_re, bar_im, bb_re, bb_im = coefficients(decay_log, phase, b_real, b_imag)
    in_re = jnp.einsum("tgh,gph->tgp", drive, bb_re, precision=HIGHEST_PREC)
    in_im = jnp.einsum("tgh,gph->tgp", drive, bb_im, precision=HIGHEST_PREC)
    positions = jnp.arange(row_total, dtype=jnp.float32)
    back_re, back_im = powers(decay_log, phase, row_total - 1.0 - positions)
    end_re = jnp.sum(back_re * in_re - back_im * in_im, axis=0)
    end_im = jnp.sum(back_re * in_im + back_im * in_re, axis=0)
    whole_re, whole_im = powers(decay_log, phase, jnp.full((1,), row_total, jnp.float32))
    unity = jnp.ones_like(end_re)
    nothing = jnp.zeros_like(end_re)
    carried = entering(
        (whole_re[0], whole_im[0], end_re, end_im),
        "sp",
        combine,
        (unity, nothing, nothing, nothing),
    )
    held_re, held_im = (carried[2], carried[3])
    seeded_re = in_re.at[0].add(bar_re * held_re - bar_im * held_im)
    seeded_im = in_im.at[0].add(bar_re * held_im + bar_im * held_re)
    total_re, total_im = prefix_states(seeded_re, seeded_im, bar_re, bar_im)
    mixed_pre = readout(total_re, total_im, c_real, c_imag) + skip_gain.reshape(groups, -1) * drive
    z_local = jax.nn.gelu(mixed_pre).reshape(row_total, width).astype(jnp.bfloat16)
    shard_rows = lax.all_gather(z_local, "tp", axis=1, tiled=True)
    projected_value = jnp.dot(shard_rows, w_value, preferred_element_type=jnp.float32)
    projected_gate = jnp.dot(shard_rows, w_gate, preferred_element_type=jnp.float32)
    gated = projected_value * jax.nn.sigmoid(projected_gate)
    squares = lax.psum(jnp.sum(gated * gated, axis=1), "tp")
    scale = lax.rsqrt(squares / D + NORM_EPS)
    return (gated * scale[:, None] * norm_out).astype(jnp.bfloat16)


def solution(mesh):
    placed = (
        P(("sp", "tp"), None),
        P(),
        P("tp", None),
        P("tp", None),
        P("tp", None, None),
        P("tp", None, None),
        P("tp", None, None),
        P("tp", None, None),
        P("tp"),
        P(None, "tp"),
        P(None, "tp"),
        P("tp"),
    )
    return jax.shard_map(
        on_device, mesh=mesh, in_specs=placed, out_specs=P("sp", "tp"), check_vma=False
    )
```

profile of v0, /device:TPU:0, one launch (start us, length us, event | category | flops | bytes accessed | tf_op | source)
XLA Modules:
  0.0 203.8 jit_solution(2601990353164014799)
XLA Ops:
  0.0 0.0 copy-start
  0.0 1.2 fusion.47
  1.2 1.1 fusion.49
  2.3 0.7 copy.38
  3.0 4.2 %all-to-all-start = ((bf16[48,4,512]{2,0,1:T(8,128)(2,1)}), bf16[48,4,512]{2,0,1:T(8,128)(2,1)S(1)}, u32[]{:S(2)}, u32[]{:S(2)}) async-start(bf16[48,4,512]{2,0,1:T(8,128)(2,1)} %bitcast.63), calls=%async_computation | async-start | bytes 393216 | tf_op jit(solution)/shard_map/all_to_all | solution.py:96
  7.2 1.5 multiply_subtract_fusion.6
  8.7 1.4 fusion.62
  10.1 31.6 %all-gather = f32[256,64]{1,0:T(8,128)S(1)} all-gather(f32[32,64]{1,0:T(8,128)S(1)} %get-tuple-element.252), channel_id=2, replica_groups=mesh['sp'=8,'tp'=4] {'sp'}, dimensions={0}, use_global_device_ids=true | all-gather | bytes 73728 | tf_op jit(solution)/shard_map/all_gather | solution.py:15
  41.7 1.4 mul.652
  43.1 30.5 %all-gather.1 = f32[256,64]{1,0:T(8,128)S(1)} all-gather(f32[32,64]{1,0:T(8,128)S(1)} %get-tuple-element.251), channel_id=3, replica_groups=mesh['sp'=8,'tp'=4] {'sp'}, dimensions={0}, use_global_device_ids=true | all-gather | bytes 73728 | tf_op jit(solution)/shard_map/all_gather | solution.py:15
  73.6 0.5 iota_subtract_fusion
  74.1 0.0 all-to-all-done
  74.1 0.3 copy.33
  74.4 0.3 reshape.121
  74.7 0.0 copy-start.3
  74.8 0.0 copy-start.16
  74.8 0.0 copy-start.17
  74.8 0.0 copy-start.18
  74.8 0.0 copy-start.19
  74.8 0.0 copy-start.22
  74.8 0.0 copy-done.2
  74.8 2.1 %fusion.54 = f32[32,64,192]{2,1,0:T(8,128)S(1)} fusion(bf16[192,32,16]{0,2,1:T(8,128)(2,1)S(1)} %reshape.121, f32[32,64,16]{1,2,0:T(8,128)S(1)} %copy-done.2, f32[32,64,16]{1,2,0:T(8,128)} %param.22, f32[32,64]{1,0:T(8,128)} %get-tuple-element.250, f32[32,64]{1,0:T(8,128)} %get-tuple-element.249), kind=kOutput, calls=%fused_computation.81 | convolution fusion | flops 75595776 | bytes 2048000 | tf_op jit(solution)/shard_map/tgh,gph->tgp/dot_general | solution.py:101
  76.9 0.0 copy-done.3
  76.9 0.0 copy-done.16
  76.9 0.0 copy-done.17
  76.9 0.0 copy-done.18
  76.9 0.0 copy-done.19
  77.0 0.0 copy-done.22
  77.0 0.0 copy-start.1
  77.0 13.3 %add_reduce_fusion = (f32[32,64]{1,0:T(8,128)S(1)}, f32[32,64]{1,0:T(8,128)S(1)}, f32[32,64,192]{2,1,0:T(8,128)}) fusion(f32[32,64]{1,0:T(8,128)S(1)} %copy-done.18, f32[32,64]{1,0:T(8,128)S(1)} %copy-done.19, f32[192]{0:T(256)S(1)} %copy-done.22, f32[32,64,192]{2,1,0:T(8,128)S(1)} %fusion.54, bf16[192,32,16]{0,2,1:T(8,128)(2,1)S(1)} %reshape.121, ...), kind=kOutput, calls=%fused_computation.44 | convolution fusion | flops 80310272 | bytes 3654400 | tf_op jit(solution)/shard_map/tgh,gph->tgp/dot_general | solution.py:102
  90.3 0.0 copy-done.1
  90.3 30.5 %all-gather.2 = f32[256,64]{1,0:T(8,128)S(1)} all-gather(f32[32,64]{1,0:T(8,128)S(1)} %get-tuple-element.199), channel_id=4, replica_groups=mesh['sp'=8,'tp'=4] {'sp'}, dimensions={0}, use_global_device_ids=true | all-gather | bytes 73728 | tf_op jit(solution)/shard_map/all_gather | solution.py:15
  120.8 30.7 %all-gather.3 = f32[256,64]{1,0:T(8,128)S(1)} all-gather(f32[32,64]{1,0:T(8,128)S(1)} %get-tuple-element.198), channel_id=5, replica_groups=mesh['sp'=8,'tp'=4] {'sp'}, dimensions={0}, use_global_device_ids=true | all-gather | bytes 73728 | tf_op jit(solution)/shard_map/all_gather | solution.py:15
  151.5 0.3 while.18
  151.8 2.2 %slice_reduce_fusion = (f32[32,64]{1,0:T(8,128)S(1)}, f32[32,64]{1,0:T(8,128)S(1)}) fusion(f32[32,64,192]{2,1,0:T(8,128)} %get-tuple-element.253, f32[32,64,192]{2,1,0:T(8,128)} %copy-done.1), kind=kLoop, calls=%fused_computation.55 | loop fusion | bytes 32768 | tf_op jit(solution)/shard_map/slice.55
  154.0 1.4 copy.34
  155.4 0.4 copy.35
  155.8 3.7 %scatter-add.6 = f32[192,32,64]{0,2,1:T(8,128)} dynamic-update-slice(f32[192,32,64]{0,2,1:T(8,128)} %bitcast.82, f32[1,32,64]{0,2,1:T(8,128)} %copy.34, s32[]{:T(128)} %constant.103.clone.1, s32[]{:T(128)} %constant.103.clone.1, s32[]{:T(128)} %constant.103.clone.1) | dynamic-update-slice | bytes 16388 | tf_op jit(solution)/shard_map/scatter-add | solution.py:117
  159.5 3.5 %scatter-add.9 = f32[192,32,64]{0,2,1:T(8,128)} dynamic-update-slice(f32[192,32,64]{0,2,1:T(8,128)} %bitcast.94, f32[1,32,64]{0,2,1:T(8,128)S(1)} %copy.35, s32[]{:T(128)} %constant.103.clone.1, s32[]{:T(128)} %constant.103.clone.1, s32[]{:T(128)} %constant.103.clone.1) | dynamic-update-slice | bytes 16388 | tf_op jit(solution)/shard_map/scatter-add | solution.py:118
  163.0 5.3 %multiply_add_fusion.5 = (f32[192,32,64]{0,2,1:T(8,128)S(1)}, f32[192,32,64]{0,2,1:T(8,128)S(1)}) fusion(f32[192,32,64]{0,2,1:T(8,128)} %scatter-add.9, f32[191,32,64]{0,2,1:T(8,128)} %bitcast.95, f32[191,32,64]{0,2,1:T(8,128)} %bitcast.83, f32[32,64]{1,0:T(8,128)S(1)} %get-tuple-element.230, f32[32,64]{1,0:T(8,128)S(1)} %get-tuple-element.229, ...), kind=kLoop, calls=%fused_computation.42 | loop fusion | flops 3145728 | bytes 9437184 | tf_op jit(solution)/shard_map/add | solution.py:48
  168.3 0.0 copy-done.13
  168.4 0.0 copy-done.14
  168.4 0.0 copy-start.11
  168.4 1.9 multiply_add_fusion.4
  170.4 1.9 multiply_add_fusion.3
  172.3 1.9 multiply_add_fusion.2
  174.3 1.9 multiply_add_fusion.1
  176.2 1.9 multiply_add_fusion
  178.2 0.1 slice.124
  178.3 0.1 slice.125
  178.4 1.9 fusion.6
  180.3 0.0 copy-start.4
  180.3 0.1 slice.126
  180.4 0.1 slice.127
  180.5 0.8 copy-done.4
  181.2 1.8 fusion.10
  183.1 0.0 copy-start.21
  183.1 2.0 fusion.44
  185.1 10.5 %all_gather.27 = bf16[192,2048]{0,1:T(8,128)(2,1)S(1)} all-gather(bf16[192,512]{0,1:T(8,128)(2,1)S(1)} %bitcast.96), channel_id=1, replica_groups=mesh['sp'=8,'tp'=4] {'tp'}, dimensions={1}, use_global_device_ids=true | all-gather | bytes 983040 | tf_op jit(solution)/shard_map/all_gather | solution.py:122
  195.6 0.7 fusion.30
  196.3 0.0 copy-start.20
  196.3 0.7 multiply_reduce_fusion
  197.0 6.0 %psum.7 = f32[192]{0:T(256)S(1)} all-reduce(f32[192]{0:T(256)S(1)} %get-tuple-element.254), channel_id=1, replica_groups=mesh['sp'=8,'tp'=4] {'tp'}, use_global_device_ids=true, to_apply=%region_6.7 | all-reduce | flops 192 | bytes 1536 | tf_op jit(solution)/shard_map/psum | solution.py:126
  203.0 0.8 multiply_convert_fusion
  (36 shorter events, 0.2 us)
Async XLA Ops:
  0.0 196.3 %copy-start = (bf16[2048,512]{1,0:T(8,128)(2,1)S(1)}, bf16[2048,512]{1,0:T(8,128)(2,1)}, u32[]{:S(2)}) copy-start(bf16[2048,512]{1,0:T(8,128)(2,1)} %param.27) | copy-start | bytes 6291460
  0.0 74.8 %copy-start.2 = (f32[32,64,16]{1,2,0:T(8,128)S(1)}, f32[32,64,16]{1,2,0:T(8,128)}, u32[]{:S(2)}) copy-start(f32[32,64,16]{1,2,0:T(8,128)} %param.23) | copy-start | bytes 393220
  3.0 71.1 %all-to-all-start = ((bf16[48,4,512]{2,0,1:T(8,128)(2,1)}), bf16[48,4,512]{2,0,1:T(8,128)(2,1)S(1)}, u32[]{:S(2)}, u32[]{:S(2)}) async-start(bf16[48,4,512]{2,0,1:T(8,128)(2,1)} %bitcast.63), calls=%async_computation | async-start | bytes 393216 | tf_op jit(solution)/shard_map/all_to_all | solution.py:96
  74.7 2.2 %copy-start.3 = (f32[32,64,16]{1,2,0:T(8,128)S(1)}, f32[32,64,16]{1,2,0:T(8,128)}, u32[]{:S(2)}) copy-start(f32[32,64,16]{1,2,0:T(8,128)} %param.22) | copy-start | bytes 393220
  74.8 2.2 %copy-start.16 = (f32[32,64]{1,0:T(8,128)S(1)}, f32[32,64]{1,0:T(8,128)}, u32[]{:S(2)}) copy-start(f32[32,64]{1,0:T(8,128)} %get-tuple-element.249) | copy-start | bytes 24580
  74.8 2.2 %copy-start.17 = (f32[32,64]{1,0:T(8,128)S(1)}, f32[32,64]{1,0:T(8,128)}, u32[]{:S(2)}) copy-start(f32[32,64]{1,0:T(8,128)} %get-tuple-element.250) | copy-start | bytes 24580
  74.8 2.2 %copy-start.18 = (f32[32,64]{1,0:T(8,128)S(1)}, f32[32,64]{1,0:T(8,128)}, u32[]{:S(2)}) copy-start(f32[32,64]{1,0:T(8,128)} %param.21) | copy-start | bytes 24580
  74.8 2.2 %copy-start.19 = (f32[32,64]{1,0:T(8,128)S(1)}, f32[32,64]{1,0:T(8,128)}, u32[]{:S(2)}) copy-start(f32[32,64]{1,0:T(8,128)} %param.20) | copy-start | bytes 24580
  74.8 2.2 %copy-start.22 = (f32[192]{0:T(256)S(1)}, f32[192]{0:T(256)}, u32[]{:S(2)}) copy-start(f32[192]{0:T(256)} %iota_subtract_fusion) | copy-start | bytes 2308
  77.0 13.3 %copy-start.1 = (f32[32,64,192]{2,1,0:T(8,128)}, f32[32,64,192]{2,1,0:T(8,128)S(1)}, u32[]{:S(2)}) copy-start(f32[32,64,192]{2,1,0:T(8,128)S(1)} %fusion.54) | copy-start | bytes 4718596
  163.0 5.3 %copy-start.13 = (f32[32,64]{1,0:T(8,128)S(1)}, f32[32,64]{1,0:T(8,128)}, u32[]{:S(2)}) copy-start(f32[32,64]{1,0:T(8,128)} %get-tuple-element.227) | copy-start | bytes 24580
  163.0 5.3 %copy-start.14 = (f32[32,64]{1,0:T(8,128)S(1)}, f32[32,64]{1,0:T(8,128)}, u32[]{:S(2)}) copy-start(f32[32,64]{1,0:T(8,128)} %get-tuple-element.228) | copy-start | bytes 24580
  168.4 2.0 copy-start.11
  168.4 2.0 copy-start.12
  170.3 2.0 copy-start.9
  170.3 2.0 copy-start.10
  172.3 2.0 copy-start.7
  172.3 2.0 copy-start.8
  174.3 1.9 copy-start.6
  180.3 1.0 copy-start.4
  181.2 1.8 copy-start.5
  181.2 1.9 copy-start.15
  183.1 12.5 %copy-start.21 = (bf16[2048,512]{1,0:T(8,128)(2,1)S(1)}, bf16[2048,512]{1,0:T(8,128)(2,1)}, u32[]{:S(2)}) copy-start(bf16[2048,512]{1,0:T(8,128)(2,1)} %param.28) | copy-start | bytes 6291460
  196.3 6.7 %copy-start.20 = (f32[512]{0:T(512)S(1)}, f32[512]{0:T(512)}, u32[]{:S(2)}) copy-start(f32[512]{0:T(512)} %param.29) | copy-start | bytes 6148
where the time goes:
time: 204 us
  blocking collectives  140 us (69%)
  other arithmetic  23.5 us (12%)
  matrix products  20.6 us (10%)
  local copies, waits for them, and re-layouts  15.1 us (7%)
  starting transfers between devices  4.24 us (2%)
    all_gather x4, blocking collectives, entering(): pieces = jax.tree.map(lambda part: lax.all_gather(part, axis), value)  123 us
    add x7, other arithmetic, prefix_states(): drive_im + rate_re * moved_im + rate_im * moved_re  16.8 us
    dot_general x1, matrix products, on_device(): in_im = jnp.einsum('tgh,gph->tgp', drive, bb_im, precision=HIGHEST_PREC)  13.3 us
    all_gather x1, blocking collectives, on_device(): shard_rows = lax.all_gather(z_local, 'tp', axis=1, tiled=True)  10.5 us
    psum x1, blocking collectives, on_device(): squares = lax.psum(jnp.sum(gated * gated, axis=1), 'tp')  6.01 us
    all_to_all x1, starting transfers between devices, on_device(): lax.all_to_all(normed, 'tp', split_axis=1, concat_axis=0, tiled=True)  4.24 us
  transfers between devices with their start and end apart: 1, of which 0 were waited for; matrix products, arithmetic and copies ran while one was open for 2% of the time, Pallas kernels for 0%

commit v1 on v0

v1 whole, which is shorter than its diff:
```python
import functools

import jax
import jax.numpy as jnp
from jax import lax
from jax.experimental import pallas as pl
from jax.experimental.pallas import tpu as pltpu
from jax.sharding import PartitionSpec as P

NORM_EPS = 1e-06
SEG = 8
LANES = 128
F32 = jnp.float32
BF16 = jnp.bfloat16
NT_DIMS = (((1,), (1,)), ((), ()))


def iota(shape, dim):
    return lax.broadcasted_iota(jnp.int32, shape, dim)


def cmul(a, b):
    return (a[0] * b[0] - a[1] * b[1], a[0] * b[1] + a[1] * b[0])


def cpow(a, n):
    result = None
    while n:
        if n & 1:
            result = a if result is None else cmul(result, a)
        n >>= 1
        if n:
            a = cmul(a, a)
    return result


def rate(decay, phase):
    magnitude = jnp.exp(decay)
    return (magnitude * jnp.cos(phase), magnitude * jnp.sin(phase))


def row(pair, index):
    shape = (SEG, LANES)
    return tuple(jnp.broadcast_to(part[index : index + 1, :], shape) for part in pair)


def norm_kernel(x_ref, gain_ref, out_ref):
    x = x_ref[...].astype(F32)
    mean = jnp.mean(x * x, axis=1, keepdims=True)
    y = (x * lax.rsqrt(mean + NORM_EPS) * gain_ref[...]).astype(BF16)
    count, _, width = out_ref.shape
    for k in range(count):
        out_ref[k] = y[:, k * width : (k + 1) * width]


def drive_tile(rows, wb_ref, k, part):
    return lax.dot_general(rows, wb_ref[k, part], NT_DIMS, preferred_element_type=F32)


def ends_kernel(u_ref, br_ref, bi_ref, decay_ref, phase_ref, up_ref, wb_ref, init_ref, end_ref, d_ref, e_ref):
    total, width = u_ref.shape
    steps = total // SEG
    tiles, _, states, _ = wb_ref.shape
    per = states // LANES
    group = br_ref.shape[1]
    entries = states * group // LANES
    r, t = iota((total, total), 0), iota((total, total), 1)
    order = (t == (r % SEG) * steps + r // SEG).astype(F32).astype(BF16)
    up_ref[...] = jnp.dot(order, u_ref[...], preferred_element_type=F32).astype(BF16)
    spread = (iota((group, LANES), 1) % group == iota((group, LANES), 0)).astype(F32).astype(BF16)
    mask = iota((states, LANES), 0) // entries == iota((states, LANES), 1) // group
    lam = rate(decay_ref[...], phase_ref[...])
    hop = cpow(lam, steps)
    hops = [hop, cmul(hop, hop)]
    hops.append(cmul(hops[1], hops[1]))
    sub = iota((SEG, LANES), 0)
    for k in range(tiles):
        for part, ref in enumerate((br_ref, bi_ref)):
            rep = jnp.dot(
                ref[k * states : (k + 1) * states, :].astype(BF16), spread, preferred_element_type=F32
            )
            wb_ref[k, part] = jnp.where(mask, rep, 0.0).astype(BF16)
            d_ref[part] = drive_tile(up_ref[:, k * LANES : (k + 1) * LANES], wb_ref, k, part)
        lams = [row(lam, k * per + m) for m in range(per)]
        x = [(d_ref[0, 0:SEG, m * LANES : (m + 1) * LANES], d_ref[1, 0:SEG, m * LANES : (m + 1) * LANES]) for m in range(per)]
        for j in range(1, steps):
            for m in range(per):
                sl = slice(m * LANES, (m + 1) * LANES)
                moved = cmul(lams[m], x[m])
                x[m] = (
                    moved[0] + d_ref[0, j * SEG : (j + 1) * SEG, sl],
                    moved[1] + d_ref[1, j * SEG : (j + 1) * SEG, sl],
                )
        for m in range(per):
            index = k * per + m
            e = x[m]
            for level in range(3):
                d = 1 << level
                back = tuple(jnp.where(sub >= d, pltpu.roll(part, d, 0), 0.0) for part in e)
                add = cmul(row(hops[level], index), back)
                e = (e[0] + add[0], e[1] + add[1])
            pairs = tiles * per
            for part in range(2):
                init_ref[part, index] = jnp.where(sub >= 1, pltpu.roll(e[part], 1, 0), 0.0)
                e_ref[part * pairs + index : part * pairs + index + 1, :] = e[part][SEG - 1 : SEG, :]
    ends = e_ref[...]
    for n in range(end_ref.shape[0]):
        end_ref[n] = ends


def mixer_kernel(
    mine_ref, up_ref, wb_ref, init_ref, end_ref, cr_ref, ci_ref, gdecay_ref, gphase_ref,
    decay_ref, phase_ref, skip_ref, z_ref, d_ref, s_ref, cw_ref, zp_ref,
):
    total, width = up_ref.shape
    steps = total // SEG
    tiles, _, states, _ = wb_ref.shape
    per = states // LANES
    pairs = tiles * per
    entries = cr_ref.shape[1]
    groups = gdecay_ref.shape[0]
    group = cr_ref.shape[0] // groups
    each = LANES // group
    gd, gp = gdecay_ref[...], gphase_ref[...]
    gbar = rate(gd, gp)
    modulus = gd * gd + gp * gp
    coef_re = ((gbar[0] - 1.0) * gd + gbar[1] * gp) / modulus
    coef_im = (gbar[1] * gd - (gbar[0] - 1.0) * gp) / modulus
    lam = rate(decay_ref[...], phase_ref[...])
    hop = cpow(lam, steps)
    hop2 = cmul(hop, hop)
    hop4 = cmul(hop2, hop2)
    whole = cmul(hop4, hop4)

    def join(i, held):
        moved = cmul(whole, held)
        return (moved[0] + end_ref[i, 0:pairs, :], moved[1] + end_ref[i, pairs : 2 * pairs, :])

    nothing = jnp.zeros((pairs, LANES), F32)
    held = lax.fori_loop(0, mine_ref[0], join, (nothing, nothing))
    sub = iota((SEG, LANES), 0)
    for k in range(tiles):
        rows = up_ref[:, k * LANES : (k + 1) * LANES]
        for part in range(2):
            d_ref[part] = drive_tile(rows, wb_ref, k, part)
        cw_ref[...] = jnp.zeros(cw_ref.shape, BF16)
        blank = jnp.zeros((group, entries), F32)
        for q in range(each):
            g = k * each + q
            cr = cr_ref[g * group : (g + 1) * group, :]
            ci = ci_ref[g * group : (g + 1) * group, :]
            fr, fi = coef_re[g : g + 1, :], coef_im[g : g + 1, :]
            per_vreg = LANES // entries
            m, slot = q // per_vreg, q % per_vreg
            for part, value in enumerate((cr * fr - ci * fi, -(cr * fi + ci * fr))):
                wide = jnp.concatenate([value if n == slot else blank for n in range(per_vreg)], axis=1)
                start = part * states + m * LANES
                cw_ref[q * group : (q + 1) * group, start : start + LANES] = wide.astype(BF16)
        lams, x = [], []
        for m in range(per):
            index = k * per + m
            lams.append(row(lam, index))
            power = (jnp.ones((SEG, LANES), F32), jnp.zeros((SEG, LANES), F32))
            for level, value in enumerate((hop, hop2, hop4)):
                bit = (sub >> level) & 1 == 1
                more = cmul(power, row(value, index))
                power = tuple(jnp.where(bit, a, b) for a, b in zip(more, power))
            seed = cmul(power, row(held, index))
            x.append((init_ref[0, index] + seed[0], init_ref[1, index] + seed[1]))
        for j in range(0, steps, 2):
            for m in range(per):
                sl = slice(m * LANES, (m + 1) * LANES)
                two = []
                for i in (j, j + 1):
                    moved = cmul(lams[m], x[m])
                    x[m] = (
                        moved[0] + d_ref[0, i * SEG : (i + 1) * SEG, sl],
                        moved[1] + d_ref[1, i * SEG : (i + 1) * SEG, sl],
                    )
                    two.append(x[m])
                for part in range(2):
                    start = part * states + m * LANES
                    s_ref[j * SEG : (j + 2) * SEG, start : start + LANES] = jnp.concatenate(
                        [two[0][part], two[1][part]], axis=0
                    ).astype(BF16)
        y = lax.dot_general(s_ref[...], cw_ref[...], NT_DIMS, preferred_element_type=F32)
        y = y + skip_ref[:, k * LANES : (k + 1) * LANES] * rows.astype(F32)
        zp_ref[:, k * LANES : (k + 1) * LANES] = jax.nn.gelu(y).astype(BF16)
    t, r = iota((total, total), 0), iota((total, total), 1)
    order = (t == (r % SEG) * steps + r // SEG).astype(F32).astype(BF16)
    z_ref[...] = jnp.dot(order, zp_ref[...], preferred_element_type=F32).astype(BF16)


def on_device(
    tokens, norm_in, decay_log, phase, b_real, b_imag, c_real, c_imag, skip_gain, w_value, w_gate, norm_out
):
    n_sp, n_tp = lax.axis_size("sp"), lax.axis_size("tp")
    rows_own, features = tokens.shape
    width = features // n_tp
    total = rows_own * n_tp
    groups, entries = decay_log.shape
    group = width // groups
    tiles = width // LANES
    states = LANES // group * entries
    pairs = groups * entries // LANES
    shape = jax.ShapeDtypeStruct
    limit = pltpu.CompilerParams(vmem_limit_bytes=40 * 1024 * 1024)
    normed = pl.pallas_call(norm_kernel, out_shape=shape((n_tp, rows_own, width), BF16))(
        tokens, norm_in.reshape(1, features)
    )
    mine = lax.all_to_all(normed, "tp", split_axis=0, concat_axis=0, tiled=True)
    u = mine.reshape(total, width)
    lane_decay = decay_log.reshape(pairs, LANES)
    lane_phase = phase.reshape(pairs, LANES)
    up, wb, init, ends = pl.pallas_call(
        ends_kernel,
        out_shape=(
            shape((total, width), BF16),
            shape((tiles, 2, states, LANES), BF16),
            shape((2, pairs, SEG, LANES), F32),
            shape((n_sp, 2 * pairs, LANES), F32),
        ),
        scratch_shapes=[pltpu.VMEM((2, total, states), F32), pltpu.VMEM((2 * pairs, LANES), F32)],
        compiler_params=limit,
    )(
        u,
        b_real.reshape(groups * entries, group),
        b_imag.reshape(groups * entries, group),
        lane_decay,
        lane_phase,
    )
    others = lax.all_to_all(ends, "sp", split_axis=0, concat_axis=0, tiled=True)
    vmem = pl.BlockSpec(memory_space=pltpu.VMEM)
    z = pl.pallas_call(
        mixer_kernel,
        out_shape=shape((total, width), BF16),
        in_specs=[pl.BlockSpec(memory_space=pltpu.SMEM)] + [vmem] * 11,
        scratch_shapes=[
            pltpu.VMEM((2, total, states), F32),
            pltpu.VMEM((total, 2 * states), BF16),
            pltpu.VMEM((LANES, 2 * states), BF16),
            pltpu.VMEM((total, width), BF16),
        ],
        compiler_params=limit,
    )(
        lax.axis_index("sp").astype(jnp.int32).reshape(1),
        up,
        wb,
        init,
        others,
        c_real.reshape(width, entries),
        c_imag.reshape(width, entries),
        decay_log,
        phase,
        lane_decay,
        lane_phase,
        skip_gain.reshape(1, width),
    )
    z_all = lax.all_gather(z, "tp", axis=1, tiled=True)
    value = jnp.dot(z_all, w_value, preferred_element_type=F32)
    gate = jnp.dot(z_all, w_gate, preferred_element_type=F32)
    gated = value * jax.nn.sigmoid(gate)
    squares = lax.psum(jnp.sum(gated * gated, axis=1), "tp")
    scale = lax.rsqrt(squares / features + NORM_EPS)
    return (gated * scale[:, None] * norm_out).astype(BF16)


def solution(mesh):
    placed = (
        P(("sp", "tp"), None),
        P(),
        P("tp", None),
        P("tp", None),
        P("tp", None, None),
        P("tp", None, None),
        P("tp", None, None),
        P("tp", None, None),
        P("tp"),
        P(None, "tp"),
        P(None, "tp"),
        P("tp"),
    )
    return jax.shard_map(on_device, mesh=mesh, in_specs=placed, out_specs=P("sp", "tp"), check_vma=False)
```

time: 204 us -> 56.9 us (0.28)
  blocking collectives: 140 us -> 14.8 us
  other arithmetic: 23.5 us -> 0.79 us
  matrix products: 20.6 us -> 1.31 us
  waiting for transfers between devices: 0.01 us -> 7.65 us
  starting transfers between devices: 4.24 us -> 10.7 us
  Pallas kernels: 0 us -> 5.92 us
    all_gather x5 -> x1, blocking collectives: 134 us -> 8.82 us  [on_device(): z_all = lax.all_gather(z, 'tp', axis=1, tiled=True)]
    dot_general x6 -> x2, matrix products: 20.6 us -> 1.31 us  [the longest x1 0.74 us: on_device(): gate = jnp.dot(z_all, w_gate, preferred_element_type=F32)]
    add x8 -> x0, other arithmetic: 16.8 us -> none  [the longest x7 16.8 us: prefix_states(): drive_im + rate_re * moved_im + rate_im * moved_re]
    unnamed x46 -> x30, local copies, waits for them, and re-layouts: 0.87 us -> 13.3 us
    all_to_all x1 -> x2, waiting for transfers between devices: 0.01 us -> 7.65 us  [the longest x1 7.52 us: on_device(): others = lax.all_to_all(ends, 'sp', split_axis=0, concat_axis=0, tiled=True)]
    scatter-add x2 -> x0, local copies, waits for them, and re-layouts: 7.25 us -> none  [the longest x1 3.72 us: on_device(): seeded_re = in_re.at[0].add(bar_re * held_re - bar_im * held_im)]
    all_to_all x1 -> x2, starting transfers between devices: 4.24 us -> 10.7 us  [the longest x1 6.42 us: on_device(): others = lax.all_to_all(ends, 'sp', split_axis=0, concat_axis=0, tiled=True)]
    pallas_call x0 -> x3, Pallas kernels: none -> 5.92 us  [the longest x1 2.21 us: on_device(): pl.pallas_call(ends_kernel, out_shape=(shape((total, width), BF16), shape...]
  transfers between devices with their start and end apart: 1 -> 2, of which waited for: 0 -> 2; matrix products, arithmetic and copies ran while one was open for 2% -> 9% of each run, Pallas kernels for 0% -> 0%
where the time goes in v1:
time: 56.9 us; the launch traced here: 56.1 us
  local copies, waits for them, and re-layouts  14.8 us (26%)
  blocking collectives  14.8 us (26%)
  starting transfers between devices  10.7 us (19%)
  waiting for transfers between devices  7.65 us (13%)
  Pallas kernels  5.92 us (10%)
  matrix products  1.31 us (2%)
  other arithmetic  0.79 us (1%)
    unnamed x30, local copies, waits for them, and re-layouts  13.3 us
    all_gather x1, blocking collectives, on_device(): z_all = lax.all_gather(z, 'tp', axis=1, tiled=True)  8.82 us
    all_to_all x1, waiting for transfers between devices, on_device(): others = lax.all_to_all(ends, 'sp', split_axis=0, concat_axis=0, tiled=True)  7.52 us
    all_to_all x1, starting transfers between devices, on_device(): others = lax.all_to_all(ends, 'sp', split_axis=0, concat_axis=0, tiled=True)  6.42 us
    psum x1, blocking collectives, on_device(): squares = lax.psum(jnp.sum(gated * gated, axis=1), 'tp')  6 us
    all_to_all x1, starting transfers between devices, on_device(): mine = lax.all_to_all(normed, 'tp', split_axis=0, concat_axis=0, tiled=True)  4.24 us
    pallas_call x1, Pallas kernels, on_device(): pl.pallas_call(ends_kernel, out_shape=(shape((total, width), BF16), shape...  2.21 us
    pallas_call x1, Pallas kernels, on_device(): pl.pallas_call(norm_kernel, out_shape=shape((n_tp, rows_own, width), BF16))  1.89 us
  transfers between devices with their start and end apart: 2, of which 2 were waited for; matrix products, arithmetic and copies ran while one was open for 9% of the time, Pallas kernels for 0%

profile of v1, /device:TPU:0, one launch (start us, length us, event | category | flops | bytes accessed | tf_op | source)
XLA Modules:
  0.0 56.1 jit_solution(4719925609330572312)
XLA Ops:
  0.0 0.0 copy-start
  0.0 1.9 %shard_map.118 = bf16[4,48,512]{2,1,0:T(8,128)(2,1)} custom-call(bf16[48,2048]{1,0:T(8,128)(2,1)} %x_ref.1, f32[1,2048]{1,0:T(1,128)} %bitcast.18), custom_call_target="tpu_custom_call" | custom-call | tf_op jit(solution)/shard_map/pallas_call | solution.py:208
  1.9 4.2 %all-to-all-start = ((bf16[4,48,512]{2,1,0:T(8,128)(2,1)}), bf16[4,48,512]{2,1,0:T(8,128)(2,1)S(1)}, u32[]{:S(2)}, u32[]{:S(2)}) async-start(bf16[4,48,512]{2,1,0:T(8,128)(2,1)} %shard_map.118), calls=%async_computation | async-start | bytes 393216 | tf_op jit(solution)/shard_map/all_to_all | solution.py:211
  6.1 0.8 %reshape.37.decay_ref = f32[16,128]{1,0:T(8,128)S(1)} reshape(f32[32,64]{1,0:T(8,128)} %gdecay_ref.1) | data formatting | bytes 16384 | tf_op jit(solution)/shard_map/reshape | solution.py:213
  6.9 0.8 %reshape.38.phase_ref = f32[16,128]{1,0:T(8,128)S(1)} reshape(f32[32,64]{1,0:T(8,128)} %gphase_ref.1) | data formatting | bytes 16384 | tf_op jit(solution)/shard_map/reshape | solution.py:214
  7.7 1.3 %copy.13 = f32[32,64,16]{2,1,0:T(8,128)S(1)} copy(f32[32,64,16]{1,2,0:T(8,128)} %param.16) | data formatting | bytes 262144 | tf_op args[4]
  9.0 2.3 %copy.14 = f32[32,64,16]{2,1,0:T(8,128)} copy(f32[32,64,16]{1,2,0:T(8,128)} %param.17) | data formatting | bytes 262144 | tf_op args[5]
  11.3 0.1 all-to-all-done
  11.4 0.0 copy-start.1
  11.4 1.2 %copy-done.1 = f32[32,64,16]{2,1,0:T(8,128)S(1)} copy-done((f32[32,64,16]{2,1,0:T(8,128)S(1)}, f32[32,64,16]{2,1,0:T(8,128)}, u32[]{:S(2)}) %copy-start.1) | copy-done | bytes 131096
  12.7 2.2 %shard_map.119 = (bf16[192,512]{1,0:T(8,128)(2,1)S(1)}, bf16[4,2,512,128]{3,2,1,0:T(8,128)(2,1)S(1)}, f32[2,16,8,128]{3,2,1,0:T(8,128)S(1)}, f32[8,32,128]{2,1,0:T(8,128)S(1)}) custom-call(bf16[192,512]{1,0:T(8,128)(2,1)S(1)} %bitcast.14, f32[2048,16]{1,0:T(8,128)S(1)} %bitcast.12, f32[2048,16]{1,0:T(8,128)S(1)} %bitcast.13, ...), custom_call_target="tpu_custom_call" | custom-call | tf_op jit(solution)/shard_map/pallas_call | solution.py:215
  14.9 0.0 copy-start.2
  14.9 1.0 %copy-done.2 = bf16[4,2,512,128]{3,2,1,0:T(8,128)(2,1)} copy-done((bf16[4,2,512,128]{3,2,1,0:T(8,128)(2,1)}, bf16[4,2,512,128]{3,2,1,0:T(8,128)(2,1)S(1)}, u32[]{:S(2)}) %copy-start.2) | copy-done | bytes 1048600
  15.9 0.0 copy-start.6
  15.9 0.7 %copy-done.6 = f32[2,16,8,128]{3,2,1,0:T(8,128)} copy-done((f32[2,16,8,128]{3,2,1,0:T(8,128)}, f32[2,16,8,128]{3,2,1,0:T(8,128)S(1)}, u32[]{:S(2)}) %copy-start.6) | copy-done | bytes 131096
  16.5 0.0 copy-start.8
  16.5 0.6 %copy-done.8 = f32[8,32,128]{2,1,0:T(8,128)} copy-done((f32[8,32,128]{2,1,0:T(8,128)}, f32[8,32,128]{2,1,0:T(8,128)S(1)}, u32[]{:S(2)}) %copy-start.8) | copy-done | bytes 131096
  17.2 6.4 %all-to-all-start.1 = ((f32[8,32,128]{2,1,0:T(8,128)}), f32[8,32,128]{2,1,0:T(8,128)S(1)}, u32[]{:S(2)}, u32[]{:S(2)}) async-start(f32[8,32,128]{2,1,0:T(8,128)} %copy-done.8), calls=%async_computation.1 | async-start | bytes 262144 | tf_op jit(solution)/shard_map/all_to_all | solution.py:232
  23.6 7.5 %all-to-all-done.1.end_ref = f32[8,32,128]{2,1,0:T(8,128)S(1)} async-done(((f32[8,32,128]{2,1,0:T(8,128)}), f32[8,32,128]{2,1,0:T(8,128)S(1)}, u32[]{:S(2)}, u32[]{:S(2)}) %all-to-all-start.1) | async-done | bytes 131104 | tf_op jit(solution)/shard_map/all_to_all | solution.py:232
  31.1 0.0 copy-start.3
  31.1 1.2 %copy-done.3 = bf16[4,2,512,128]{3,2,1,0:T(8,128)(2,1)S(1)} copy-done((bf16[4,2,512,128]{3,2,1,0:T(8,128)(2,1)S(1)}, bf16[4,2,512,128]{3,2,1,0:T(8,128)(2,1)}, u32[]{:S(2)}) %copy-start.3) | copy-done | bytes 1048600
  32.3 0.0 copy-start.4
  32.3 0.9 %copy-done.4 = f32[32,16,64]{2,1,0:T(8,128)S(1)} copy-done((f32[32,16,64]{2,1,0:T(8,128)S(1)}, f32[32,16,64]{2,1,0:T(8,128)}, u32[]{:S(2)}) %copy-start.4) | copy-done | bytes 131096
  33.3 0.0 copy-start.5
  33.3 0.9 %copy-done.5 = f32[32,16,64]{2,1,0:T(8,128)S(1)} copy-done((f32[32,16,64]{2,1,0:T(8,128)S(1)}, f32[32,16,64]{2,1,0:T(8,128)}, u32[]{:S(2)}) %copy-start.5) | copy-done | bytes 131096
  34.2 0.0 copy-start.7
  34.2 0.9 %copy-done.7 = f32[2,16,8,128]{3,2,1,0:T(8,128)S(1)} copy-done((f32[2,16,8,128]{3,2,1,0:T(8,128)S(1)}, f32[2,16,8,128]{3,2,1,0:T(8,128)}, u32[]{:S(2)}) %copy-start.7) | copy-done | bytes 131096
  35.1 0.0 copy-start.9
  35.1 0.7 %copy-done.9 = f32[32,64]{1,0:T(8,128)S(1)} copy-done((f32[32,64]{1,0:T(8,128)S(1)}, f32[32,64]{1,0:T(8,128)}, u32[]{:S(2)}) %copy-start.9) | copy-done | bytes 8216
  35.9 0.0 copy-start.10
  35.9 0.7 %copy-done.10 = f32[32,64]{1,0:T(8,128)S(1)} copy-done((f32[32,64]{1,0:T(8,128)S(1)}, f32[32,64]{1,0:T(8,128)}, u32[]{:S(2)}) %copy-start.10) | copy-done | bytes 8216
  36.6 0.0 copy-start.11
  36.6 0.7 %copy-done.11 = f32[512]{0:T(512)S(1)} copy-done((f32[512]{0:T(512)S(1)}, f32[512]{0:T(512)}, u32[]{:S(2)}) %copy-start.11) | copy-done | bytes 2072
  37.3 0.0 copy-start.12
  37.3 1.8 %shard_map.120 = bf16[192,512]{1,0:T(8,128)(2,1)S(1)} custom-call(s32[1]{0:T(128)} %bitcast.mine_ref, bf16[192,512]{1,0:T(8,128)(2,1)S(1)} %get-tuple-element.9.up_ref, bf16[4,2,512,128]{3,2,1,0:T(8,128)(2,1)S(1)} %copy-done.3, f32[2,16,8,128]{3,2,1,0:T(8,128)S(1)} %copy-done.7, f32[8,32,128]{2,1,0:T(8,128)S(1)} %all-to-all-done.1.end_ref, ...), custom_call_target="tpu_custom_call" | custom-call | tf_op jit(solution)/shard_map/pallas_call | solution.py:234
  39.1 8.8 %all_gather.3 = bf16[192,2048]{1,0:T(8,128)(2,1)S(1)} all-gather(bf16[192,512]{1,0:T(8,128)(2,1)S(1)} %shard_map.120), channel_id=1, replica_groups=mesh['sp'=8,'tp'=4] {'tp'}, dimensions={1}, use_global_device_ids=true | all-gather | bytes 983040 | tf_op jit(solution)/shard_map/all_gather | solution.py:259
  47.9 0.0 copy-done.12
  47.9 0.6 %fusion.4 = f32[192,512]{1,0:T(8,128)S(1)} fusion(bf16[192,2048]{1,0:T(8,128)(2,1)S(1)} %all_gather.3, bf16[2048,512]{1,0:T(8,128)(2,1)S(1)} %copy-done.12), kind=kOutput, calls=%fused_computation.8 | convolution fusion | flops 402653184 | bytes 3276800 | tf_op jit(solution)/shard_map/dot_general | solution.py:260
  48.5 0.0 copy-done
  48.5 0.0 copy-start.13
  48.5 0.7 %multiply_reduce_fusion = (f32[192]{0:T(256)S(1)}, f32[192,512]{1,0:T(8,128)S(1)}) fusion(f32[192,512]{1,0:T(8,128)S(1)} %fusion.4, bf16[192,2048]{1,0:T(8,128)(2,1)S(1)} %all_gather.3, bf16[2048,512]{1,0:T(8,128)(2,1)S(1)} %copy-done), kind=kOutput, calls=%fused_computation.6 | convolution fusion | flops 403242816 | bytes 3670784 | tf_op jit(solution)/shard_map/dot_general | solution.py:261
  49.3 6.0 %psum.7 = f32[192]{0:T(256)S(1)} all-reduce(f32[192]{0:T(256)S(1)} %get-tuple-element.13), channel_id=1, replica_groups=mesh['sp'=8,'tp'=4] {'tp'}, use_global_device_ids=true, to_apply=%region_1.0 | all-reduce | flops 192 | bytes 1536 | tf_op jit(solution)/shard_map/psum | solution.py:263
  55.3 0.0 copy-done.13
  55.3 0.8 %multiply_convert_fusion = bf16[192,512]{1,0:T(8,128)(2,1)} fusion(f32[192,512]{1,0:T(8,128)S(1)} %get-tuple-element.14, f32[512]{0:T(512)S(1)} %copy-done.13, f32[192]{0:T(256)S(1)} %add_rsqrt_fusion), kind=kLoop, calls=%fused_computation.5 | loop fusion | flops 294912 | bytes 592640 | tf_op jit(solution)/shard_map/convert_element_type | solution.py:265
  (1 shorter events, 0.0 us)
Async XLA Ops:
  0.0 48.5 %copy-start = (bf16[2048,512]{1,0:T(8,128)(2,1)S(1)}, bf16[2048,512]{1,0:T(8,128)(2,1)}, u32[]{:S(2)}) copy-start(bf16[2048,512]{1,0:T(8,128)(2,1)} %param.22) | copy-start | bytes 6291460
  1.9 9.5 %all-to-all-start = ((bf16[4,48,512]{2,1,0:T(8,128)(2,1)}), bf16[4,48,512]{2,1,0:T(8,128)(2,1)S(1)}, u32[]{:S(2)}, u32[]{:S(2)}) async-start(bf16[4,48,512]{2,1,0:T(8,128)(2,1)} %shard_map.118), calls=%async_computation | async-start | bytes 393216 | tf_op jit(solution)/shard_map/all_to_all | solution.py:211
  11.4 1.2 %copy-start.1 = (f32[32,64,16]{2,1,0:T(8,128)S(1)}, f32[32,64,16]{2,1,0:T(8,128)}, u32[]{:S(2)}) copy-start(f32[32,64,16]{2,1,0:T(8,128)} %copy.14) | copy-start | bytes 393220
  14.9 1.0 %copy-start.2 = (bf16[4,2,512,128]{3,2,1,0:T(8,128)(2,1)}, bf16[4,2,512,128]{3,2,1,0:T(8,128)(2,1)S(1)}, u32[]{:S(2)}) copy-start(bf16[4,2,512,128]{3,2,1,0:T(8,128)(2,1)S(1)} %get-tuple-element.10.wb_ref) | copy-start | bytes 3145732
  15.9 0.7 %copy-start.6 = (f32[2,16,8,128]{3,2,1,0:T(8,128)}, f32[2,16,8,128]{3,2,1,0:T(8,128)S(1)}, u32[]{:S(2)}) copy-start(f32[2,16,8,128]{3,2,1,0:T(8,128)S(1)} %get-tuple-element.11.init_ref) | copy-start | bytes 393220
  16.5 0.7 %copy-start.8 = (f32[8,32,128]{2,1,0:T(8,128)}, f32[8,32,128]{2,1,0:T(8,128)S(1)}, u32[]{:S(2)}) copy-start(f32[8,32,128]{2,1,0:T(8,128)S(1)} %get-tuple-element.12) | copy-start | bytes 393220
  17.2 13.9 %all-to-all-start.1 = ((f32[8,32,128]{2,1,0:T(8,128)}), f32[8,32,128]{2,1,0:T(8,128)S(1)}, u32[]{:S(2)}, u32[]{:S(2)}) async-start(f32[8,32,128]{2,1,0:T(8,128)} %copy-done.8), calls=%async_computation.1 | async-start | bytes 262144 | tf_op jit(solution)/shard_map/all_to_all | solution.py:232
  31.1 1.2 %copy-start.3 = (bf16[4,2,512,128]{3,2,1,0:T(8,128)(2,1)S(1)}, bf16[4,2,512,128]{3,2,1,0:T(8,128)(2,1)}, u32[]{:S(2)}) copy-start(bf16[4,2,512,128]{3,2,1,0:T(8,128)(2,1)} %copy-done.2) | copy-start | bytes 3145732
  32.3 0.9 %copy-start.4 = (f32[32,16,64]{2,1,0:T(8,128)S(1)}, f32[32,16,64]{2,1,0:T(8,128)}, u32[]{:S(2)}) copy-start(f32[32,16,64]{2,1,0:T(8,128)} %param.18) | copy-start | bytes 393220
  33.3 0.9 %copy-start.5 = (f32[32,16,64]{2,1,0:T(8,128)S(1)}, f32[32,16,64]{2,1,0:T(8,128)}, u32[]{:S(2)}) copy-start(f32[32,16,64]{2,1,0:T(8,128)} %param.19) | copy-start | bytes 393220
  34.2 0.9 %copy-start.7 = (f32[2,16,8,128]{3,2,1,0:T(8,128)S(1)}, f32[2,16,8,128]{3,2,1,0:T(8,128)}, u32[]{:S(2)}) copy-start(f32[2,16,8,128]{3,2,1,0:T(8,128)} %copy-done.6) | copy-start | bytes 393220
  35.1 0.7 %copy-start.9 = (f32[32,64]{1,0:T(8,128)S(1)}, f32[32,64]{1,0:T(8,128)}, u32[]{:S(2)}) copy-start(f32[32,64]{1,0:T(8,128)} %gdecay_ref.1) | copy-start | bytes 24580
  35.9 0.7 %copy-start.10 = (f32[32,64]{1,0:T(8,128)S(1)}, f32[32,64]{1,0:T(8,128)}, u32[]{:S(2)}) copy-start(f32[32,64]{1,0:T(8,128)} %gphase_ref.1) | copy-start | bytes 24580
  36.6 0.7 %copy-start.11 = (f32[512]{0:T(512)S(1)}, f32[512]{0:T(512)}, u32[]{:S(2)}) copy-start(f32[512]{0:T(512)} %param.20) | copy-start | bytes 6148
  37.3 10.7 %copy-start.12 = (bf16[2048,512]{1,0:T(8,128)(2,1)S(1)}, bf16[2048,512]{1,0:T(8,128)(2,1)}, u32[]{:S(2)}) copy-start(bf16[2048,512]{1,0:T(8,128)(2,1)} %param.21) | copy-start | bytes 6291460
  48.5 6.8 %copy-start.13 = (f32[512]{0:T(512)S(1)}, f32[512]{0:T(512)}, u32[]{:S(2)}) copy-start(f32[512]{0:T(512)} %param.23) | copy-start | bytes 6148

commit v2 on v1

v2 whole, which is shorter than its diff:
```python
import jax
import jax.numpy as jnp
from jax import lax
from jax.experimental import pallas as pl
from jax.experimental.pallas import tpu as pltpu
from jax.sharding import PartitionSpec as P

NORM_EPS = 1e-06
SEG = 8
LANES = 128
TABLES = 5
F32 = jnp.float32
BF16 = jnp.bfloat16
NT_DIMS = (((1,), (1,)), ((), ()))


def iota(shape, dim):
    return lax.broadcasted_iota(jnp.int32, shape, dim)


def cmul(a, b):
    return (a[0] * b[0] - a[1] * b[1], a[0] * b[1] + a[1] * b[0])


def cpow(a, n):
    result = None
    while n:
        if n & 1:
            result = a if result is None else cmul(result, a)
        n >>= 1
        if n:
            a = cmul(a, a)
    return result


def rate(decay, phase):
    magnitude = jnp.exp(decay)
    return (magnitude * jnp.cos(phase), magnitude * jnp.sin(phase))


def wide_row(pair, index):
    shape = (SEG, LANES)
    return tuple(jnp.broadcast_to(part[index : index + 1, :], shape) for part in pair)


def table_row(tab_ref, power, index):
    shape = (SEG, LANES)
    return tuple(
        jnp.broadcast_to(tab_ref[2 * power + part, index : index + 1, :], shape) for part in range(2)
    )


def forward_order(total):
    steps = total // SEG
    r, t = iota((total, total), 0), iota((total, total), 1)
    return (t == (r % SEG) * steps + r // SEG).astype(F32).astype(BF16)


def place(ref, k, q, part, value):
    group, entries = value.shape
    fits = LANES // entries
    m, slot = q // fits, q % fits
    blank = jnp.zeros(value.shape, F32)
    wide = jnp.concatenate([value if n == slot else blank for n in range(fits)], axis=1)
    start = part * (ref.shape[2] // 2) + m * LANES
    ref[k, q * group : (q + 1) * group, start : start + LANES] = wide.astype(BF16)


def fill_tables(tab_ref, decay_ref, phase_ref, steps):
    fits = LANES // decay_ref.shape[1]
    pairs = decay_ref.shape[0] // fits
    lined = [
        jnp.concatenate([ref[pl.ds(n, pairs, stride=fits), :] for n in range(fits)], axis=1)
        for ref in (decay_ref, phase_ref)
    ]
    value = rate(*lined)
    for power in range(TABLES):
        for part in range(2):
            tab_ref[2 * power + part] = value[part]
        value = cpow(value, steps) if power == 0 else cmul(value, value)


def fetch(sources, targets, sem):
    copies = [pltpu.make_async_copy(s, t, sem.at[n]) for n, (s, t) in enumerate(zip(sources, targets))]
    for copy in copies:
        copy.start()
    return copies


def norm_kernel(x_ref, gain_ref, out_ref):
    x = x_ref[...].astype(F32)
    mean = jnp.mean(x * x, axis=1, keepdims=True)
    y = (x * lax.rsqrt(mean + NORM_EPS) * gain_ref[...]).astype(BF16)
    count, _, width = out_ref.shape
    for k in range(count):
        out_ref[k] = y[:, k * width : (k + 1) * width]


def fill_inputs(wb_ref, br_ref, bi_ref, group):
    wb_ref[...] = jnp.zeros(wb_ref.shape, BF16)
    each = LANES // group
    for k in range(wb_ref.shape[0]):
        for q in range(each):
            start = (k * each + q) * group
            for part, ref in enumerate((br_ref, bi_ref)):
                place(wb_ref, k, q, part, ref[start : start + group, :])


def weights_kernel(steps, br_hbm, bi_hbm, decay_hbm, phase_hbm, wb_ref, tab_ref, br_ref, bi_ref, decay_ref, phase_ref, sem):
    copies = fetch((decay_hbm, phase_hbm, br_hbm, bi_hbm), (decay_ref, phase_ref, br_ref, bi_ref), sem)
    copies[0].wait()
    copies[1].wait()
    fill_tables(tab_ref, decay_ref, phase_ref, steps)
    copies[2].wait()
    copies[3].wait()
    fill_inputs(wb_ref, br_ref, bi_ref, br_ref.shape[0] // decay_ref.shape[0])


def lanes_of(d_ref, part, j, m):
    half = d_ref.shape[1] // 2
    start = part * half + m * LANES
    return d_ref[j * SEG : (j + 1) * SEG, start : start + LANES]


def ends_kernel(u_ref, wb_ref, tab_ref, up_hbm, init_hbm, end_hbm, up_ref, init_ref, end_ref, d_ref, e_ref, sem):
    total = u_ref.shape[0]
    steps = total // SEG
    tiles, _, both = wb_ref.shape
    per = both // 2 // LANES
    pairs = tiles * per
    up_ref[...] = jnp.dot(forward_order(total), u_ref[...], preferred_element_type=F32).astype(BF16)
    first = fetch((up_ref,), (up_hbm,), sem)
    sub = iota((SEG, LANES), 0)
    for k in range(tiles):
        d_ref[...] = jnp.dot(up_ref[:, k * LANES : (k + 1) * LANES], wb_ref[k], preferred_element_type=F32)
        lams = [table_row(tab_ref, 0, k * per + m) for m in range(per)]
        x = [(lanes_of(d_ref, 0, 0, m), lanes_of(d_ref, 1, 0, m)) for m in range(per)]
        for j in range(1, steps):
            for m in range(per):
                moved = cmul(lams[m], x[m])
                x[m] = tuple(moved[part] + lanes_of(d_ref, part, j, m) for part in range(2))
        for m in range(per):
            index = k * per + m
            e = x[m]
            for level in range(3):
                d = 1 << level
                back = tuple(jnp.where(sub >= d, pltpu.roll(part, d, 0), 0.0) for part in e)
                add = cmul(table_row(tab_ref, 1 + level, index), back)
                e = (e[0] + add[0], e[1] + add[1])
            for part in range(2):
                init_ref[part, index] = jnp.where(sub >= 1, pltpu.roll(e[part], 1, 0), 0.0)
                e_ref[part * pairs + index : part * pairs + index + 1, :] = e[part][SEG - 1 : SEG, :]
    ends = e_ref[...]
    for n in range(end_ref.shape[0]):
        end_ref[n] = ends
    last = fetch((end_ref, init_ref), (end_hbm, init_hbm), sem.at[1:3])
    for copy in first + last:
        copy.wait()


def local_kernel(
    up_hbm, init_hbm, br_hbm, bi_hbm, cr_hbm, ci_hbm, decay_hbm, phase_hbm, skip_hbm,
    y_hbm, cw_ref, tab_ref,
    up_ref, init_ref, br_ref, bi_ref, cr_ref, ci_ref, decay_ref, phase_ref, skip_ref,
    y_ref, wb_ref, d_ref, s_ref, sem,
):
    copies = fetch(
        (up_hbm, init_hbm, br_hbm, bi_hbm, cr_hbm, ci_hbm, decay_hbm, phase_hbm, skip_hbm),
        (up_ref, init_ref, br_ref, bi_ref, cr_ref, ci_ref, decay_ref, phase_ref, skip_ref),
        sem,
    )
    for copy in copies:
        copy.wait()
    total = up_ref.shape[0]
    steps = total // SEG
    groups = decay_ref.shape[0]
    group = br_ref.shape[0] // groups
    each = LANES // group
    tiles, _, both = wb_ref.shape
    per = both // 2 // LANES
    fill_tables(tab_ref, decay_ref, phase_ref, steps)
    fill_inputs(wb_ref, br_ref, bi_ref, group)
    gd, gp = decay_ref[...], phase_ref[...]
    gbar = rate(gd, gp)
    modulus = gd * gd + gp * gp
    coef_re = ((gbar[0] - 1.0) * gd + gbar[1] * gp) / modulus
    coef_im = (gbar[1] * gd - (gbar[0] - 1.0) * gp) / modulus
    cw_ref[...] = jnp.zeros(cw_ref.shape, BF16)
    for k in range(tiles):
        for q in range(each):
            g = k * each + q
            cr = cr_ref[g * group : (g + 1) * group, :]
            ci = ci_ref[g * group : (g + 1) * group, :]
            fr, fi = coef_re[g : g + 1, :], coef_im[g : g + 1, :]
            place(cw_ref, k, q, 0, cr * fr - ci * fi)
            place(cw_ref, k, q, 1, -(cr * fi + ci * fr))
        rows = up_ref[:, k * LANES : (k + 1) * LANES]
        d_ref[...] = jnp.dot(rows, wb_ref[k], preferred_element_type=F32)
        lams = [table_row(tab_ref, 0, k * per + m) for m in range(per)]
        x = [(init_ref[0, k * per + m], init_ref[1, k * per + m]) for m in range(per)]

        def step(j, m):
            moved = cmul(lams[m], x[m])
            x[m] = tuple(moved[part] + lanes_of(d_ref, part, j, m) for part in range(2))
            return x[m]

        roll_states(s_ref, steps, per, step)
        y = lax.dot_general(s_ref[...], cw_ref[k], NT_DIMS, preferred_element_type=F32)
        y_ref[:, k * LANES : (k + 1) * LANES] = y + skip_ref[:, k * LANES : (k + 1) * LANES] * rows.astype(F32)
    last = pltpu.make_async_copy(y_ref, y_hbm, sem.at[9])
    last.start()
    last.wait()


def roll_states(s_ref, steps, per, step):
    half = s_ref.shape[1] // 2
    for j in range(0, steps, 2):
        for m in range(per):
            two = [step(j, m), step(j + 1, m)]
            for part in range(2):
                start = part * half + m * LANES
                s_ref[j * SEG : (j + 2) * SEG, start : start + LANES] = jnp.concatenate(
                    [two[0][part], two[1][part]], axis=0
                ).astype(BF16)


def carry_kernel(mine_ref, end_ref, y_hbm, cw_ref, tab_ref, z_ref, y_ref, s_ref, zp_ref, sem):
    arriving = pltpu.make_async_copy(y_hbm, y_ref, sem)
    arriving.start()
    total = y_ref.shape[0]
    steps = total // SEG
    tiles, _, both = cw_ref.shape
    per = both // 2 // LANES
    pairs = tiles * per
    whole = (tab_ref[2 * TABLES - 2], tab_ref[2 * TABLES - 1])

    def join(i, held):
        moved = cmul(whole, held)
        return (moved[0] + end_ref[i, 0:pairs, :], moved[1] + end_ref[i, pairs : 2 * pairs, :])

    nothing = jnp.zeros((pairs, LANES), F32)
    held = lax.fori_loop(0, mine_ref[0], join, (nothing, nothing))
    sub = iota((SEG, LANES), 0)
    for k in range(tiles):
        lams, x = [], []
        for m in range(per):
            index = k * per + m
            lams.append(table_row(tab_ref, 0, index))
            seed = wide_row(held, index)
            for level in range(3):
                bit = (sub >> level) & 1 == 1
                more = cmul(seed, table_row(tab_ref, 1 + level, index))
                seed = tuple(jnp.where(bit, a, b) for a, b in zip(more, seed))
            x.append(seed)

        def step(j, m):
            x[m] = cmul(lams[m], x[m])
            return x[m]

        roll_states(s_ref, steps, per, step)
        sl = slice(k * LANES, (k + 1) * LANES)
        y = lax.dot_general(s_ref[...], cw_ref[k], NT_DIMS, preferred_element_type=F32)
        if k == 0:
            arriving.wait()
        zp_ref[:, sl] = jax.nn.gelu(y + y_ref[:, sl]).astype(BF16)
    t, r = iota((total, total), 0), iota((total, total), 1)
    back = (r == (t % steps) * SEG + t // steps).astype(F32).astype(BF16)
    z_ref[...] = jnp.dot(back, zp_ref[...], preferred_element_type=F32).astype(BF16)


def on_device(
    tokens, norm_in, decay_log, phase, b_real, b_imag, c_real, c_imag, skip_gain, w_value, w_gate, norm_out
):
    n_sp, n_tp = lax.axis_size("sp"), lax.axis_size("tp")
    rows_own, features = tokens.shape
    width = features // n_tp
    total = rows_own * n_tp
    groups, entries = decay_log.shape
    group = width // groups
    tiles = width // LANES
    states = LANES // group * entries
    pairs = groups * entries // LANES
    shape = jax.ShapeDtypeStruct
    limit = pltpu.CompilerParams(vmem_limit_bytes=24 * 1024 * 1024)
    vmem = pl.BlockSpec(memory_space=pltpu.VMEM)
    smem = pl.BlockSpec(memory_space=pltpu.SMEM)
    hbm = pl.BlockSpec(memory_space=pltpu.HBM)
    wide = pltpu.VMEM((width, entries), F32)
    flat = pltpu.VMEM((groups, entries), F32)
    rows_t = ((total, width), BF16)
    init_t = ((2, pairs, SEG, LANES), F32)
    y_t = ((total, width), F32)
    ends_t = ((n_sp, 2 * pairs, LANES), F32)
    block_t = ((tiles, LANES, 2 * states), BF16)
    tab_t = ((2 * TABLES, pairs, LANES), F32)

    def held(t):
        return pltpu.VMEM(*t)

    def far(*arrays):
        return [pltpu.with_memory_space_constraint(a, pltpu.HBM) for a in arrays]

    b_re = b_real.transpose(0, 2, 1).reshape(width, entries)
    b_im = b_imag.transpose(0, 2, 1).reshape(width, entries)
    normed = pl.pallas_call(norm_kernel, out_shape=shape((n_tp, rows_own, width), BF16), name="norm")(
        tokens, norm_in.reshape(1, features)
    )
    mine = lax.all_to_all(normed, "tp", split_axis=0, concat_axis=0, tiled=True)
    u = mine.reshape(total, width)
    wb, tab = pl.pallas_call(
        lambda *refs: weights_kernel(total // SEG, *refs),
        out_shape=(pltpu.VMEM(*block_t), pltpu.VMEM(*tab_t)),
        in_specs=[hbm] * 4,
        scratch_shapes=[wide, wide, flat, flat, pltpu.SemaphoreType.DMA((4,))],
        compiler_params=limit,
        name="weights",
    )(*far(b_re, b_im, decay_log, phase))
    up, init, ends = pl.pallas_call(
        ends_kernel,
        out_shape=(pltpu.HBM(*rows_t), pltpu.HBM(*init_t), pltpu.HBM(*ends_t)),
        out_specs=(hbm, hbm, hbm),
        scratch_shapes=[
            held(rows_t),
            held(init_t),
            held(ends_t),
            pltpu.VMEM((total, 2 * states), F32),
            pltpu.VMEM((2 * pairs, LANES), F32),
            pltpu.SemaphoreType.DMA((3,)),
        ],
        compiler_params=limit,
        name="ends",
    )(u, wb, tab)
    others = lax.all_to_all(ends, "sp", split_axis=0, concat_axis=0, tiled=True)
    y, cw, tab2 = pl.pallas_call(
        local_kernel,
        out_shape=(pltpu.HBM(*y_t), pltpu.VMEM(*block_t), pltpu.VMEM(*tab_t)),
        out_specs=(hbm, vmem, vmem),
        in_specs=[hbm] * 9,
        scratch_shapes=[
            held(rows_t),
            held(init_t),
            wide,
            wide,
            wide,
            wide,
            flat,
            flat,
            pltpu.VMEM((1, width), F32),
            held(y_t),
            held(block_t),
            pltpu.VMEM((total, 2 * states), F32),
            pltpu.VMEM((total, 2 * states), BF16),
            pltpu.SemaphoreType.DMA((10,)),
        ],
        compiler_params=limit,
        name="local",
    )(
        *far(
            up,
            init,
            b_re,
            b_im,
            c_real.reshape(width, entries),
            c_imag.reshape(width, entries),
            decay_log,
            phase,
            skip_gain.reshape(1, width),
        )
    )
    z = pl.pallas_call(
        carry_kernel,
        out_shape=shape(*rows_t),
        in_specs=[smem, vmem, hbm, vmem, vmem],
        scratch_shapes=[
            held(y_t),
            pltpu.VMEM((total, 2 * states), BF16),
            held(rows_t),
            pltpu.SemaphoreType.DMA,
        ],
        compiler_params=limit,
        name="carry",
    )(lax.axis_index("sp").astype(jnp.int32).reshape(1), others, *far(y), cw, tab2)
    z_all = lax.all_gather(z, "tp", axis=1, tiled=True)
    value = jnp.dot(z_all, w_value, preferred_element_type=F32)
    gate = jnp.dot(z_all, w_gate, preferred_element_type=F32)
    gated = value * jax.nn.sigmoid(gate)
    squares = lax.psum(jnp.sum(gated * gated, axis=1), "tp")
    scale = lax.rsqrt(squares / features + NORM_EPS)
    return (gated * scale[:, None] * norm_out).astype(BF16)


def solution(mesh):
    placed = (
        P(("sp", "tp"), None),
        P(),
        P("tp", None),
        P("tp", None),
        P("tp", None, None),
        P("tp", None, None),
        P("tp", None, None),
        P("tp", None, None),
        P("tp"),
        P(None, "tp"),
        P(None, "tp"),
        P("tp"),
    )
    return jax.shard_map(on_device, mesh=mesh, in_specs=placed, out_specs=P("sp", "tp"), check_vma=False)
```

time: 56.9 us -> 46.5 us (0.82)
  local copies, waits for them, and re-layouts: 14.8 us -> 0.01 us
  Pallas kernels: 5.92 us -> 10.9 us
    unnamed x30 -> x6, local copies, waits for them, and re-layouts: 13.3 us -> 0.01 us
    pallas_call x3 -> x5, Pallas kernels: 5.92 us -> 10.9 us  [the longest x1 3.8 us: on_device(): pl.pallas_call(local_kernel, out_shape=(pltpu.HBM(*y_t), pltpu.VMEM(*bloc...]
    all_to_all x1, waiting for transfers between devices: 7.52 us -> 3.53 us  [on_device(): others = lax.all_to_all(ends, 'sp', split_axis=0, concat_axis=0, tiled=True)]
    all_to_all x1, waiting for transfers between devices: 0.13 us -> 4.01 us  [on_device(): mine = lax.all_to_all(normed, 'tp', split_axis=0, concat_axis=0, tiled=True)]
    reshape x2 -> x0, local copies, waits for them, and re-layouts: 1.57 us -> none  [the longest x1 0.79 us: on_device(): lane_phase = phase.reshape(pairs, LANES)]
    all_gather x1, blocking collectives: 8.82 us -> 7.5 us  [on_device(): z_all = lax.all_gather(z, 'tp', axis=1, tiled=True)]
    psum x1, blocking collectives: 6 us -> 7.24 us  [on_device(): squares = lax.psum(jnp.sum(gated * gated, axis=1), 'tp')]
  transfers between devices with their start and end apart: 2 -> 2, of which waited for: 2 -> 2; matrix products, arithmetic and copies ran while one was open for 9% -> 0% of each run, Pallas kernels for 0% -> 11%
where the time goes in v2:
time: 46.5 us; the launch traced here: 46.1 us
  blocking collectives  14.7 us (32%)
  Pallas kernels  10.9 us (23%)
  starting transfers between devices  10.7 us (23%)
  waiting for transfers between devices  7.54 us (16%)
  matrix products  1.32 us (3%)
  other arithmetic  0.79 us (2%)
    all_gather x1, blocking collectives, on_device(): z_all = lax.all_gather(z, 'tp', axis=1, tiled=True)  7.5 us
    psum x1, blocking collectives, on_device(): squares = lax.psum(jnp.sum(gated * gated, axis=1), 'tp')  7.24 us
    all_to_all x1, starting transfers between devices, on_device(): others = lax.all_to_all(ends, 'sp', split_axis=0, concat_axis=0, tiled=True)  6.42 us
    all_to_all x1, starting transfers between devices, on_device(): mine = lax.all_to_all(normed, 'tp', split_axis=0, concat_axis=0, tiled=True)  4.24 us
    all_to_all x1, waiting for transfers between devices, on_device(): mine = lax.all_to_all(normed, 'tp', split_axis=0, concat_axis=0, tiled=True)  4.01 us
    pallas_call x1, Pallas kernels, on_device(): pl.pallas_call(local_kernel, out_shape=(pltpu.HBM(*y_t), pltpu.VMEM(*bloc...  3.8 us
    all_to_all x1, waiting for transfers between devices, on_device(): others = lax.all_to_all(ends, 'sp', split_axis=0, concat_axis=0, tiled=True)  3.53 us
    pallas_call x1, Pallas kernels, on_device(): pl.pallas_call(carry_kernel, out_shape=shape(*rows_t), in_specs=[smem, vm...  2.28 us
  transfers between devices with their start and end apart: 2, of which 2 were waited for; matrix products, arithmetic and copies ran while one was open for 0% of the time, Pallas kernels for 11%

profile of v2, /device:TPU:0, one launch (start us, length us, event | category | flops | bytes accessed | tf_op | source)
XLA Modules:
  0.0 46.1 jit_solution(11421790915925668588)
XLA Ops:
  0.0 0.0 copy-start
  0.0 1.9 %norm.1 = bf16[4,48,512]{2,1,0:T(8,128)(2,1)} custom-call(bf16[48,2048]{1,0:T(8,128)(2,1)} %x_ref.1, f32[1,2048]{1,0:T(1,128)} %bitcast.23), custom_call_target="tpu_custom_call" | custom-call | tf_op jit(solution)/shard_map/norm/pallas_call | solution.py:305
  1.9 4.2 %all-to-all-start = ((bf16[4,48,512]{2,1,0:T(8,128)(2,1)}), bf16[4,48,512]{2,1,0:T(8,128)(2,1)S(1)}, u32[]{:S(2)}, u32[]{:S(2)}) async-start(bf16[4,48,512]{2,1,0:T(8,128)(2,1)} %norm.1), calls=%async_computation | async-start | bytes 393216 | tf_op jit(solution)/shard_map/all_to_all | solution.py:308
  6.1 1.3 %weights.1 = (bf16[4,128,1024]{2,1,0:T(8,128)(2,1)S(1)}, f32[10,16,128]{2,1,0:T(8,128)S(1)}) custom-call(f32[512,64]{1,0:T(8,128)} %bitcast.17, f32[512,64]{1,0:T(8,128)} %bitcast.19, f32[32,64]{1,0:T(8,128)} %decay_hbm.1, f32[32,64]{1,0:T(8,128)} %phase_hbm.1), custom_call_target="tpu_custom_call" | custom-call | tf_op jit(solution)/shard_map/weights/pallas_call | solution.py:310
  7.4 4.0 %all-to-all-done = bf16[4,48,512]{2,1,0:T(8,128)(2,1)S(1)} async-done(((bf16[4,48,512]{2,1,0:T(8,128)(2,1)}), bf16[4,48,512]{2,1,0:T(8,128)(2,1)S(1)}, u32[]{:S(2)}, u32[]{:S(2)}) %all-to-all-start) | async-done | bytes 196640 | tf_op jit(solution)/shard_map/all_to_all | solution.py:308
  11.4 1.7 %ends.1 = (bf16[192,512]{1,0:T(8,128)(2,1)}, f32[2,16,8,128]{3,2,1,0:T(8,128)}, f32[8,32,128]{2,1,0:T(8,128)}) custom-call(bf16[192,512]{1,0:T(8,128)(2,1)S(1)} %bitcast.16, bf16[4,128,1024]{2,1,0:T(8,128)(2,1)S(1)} %get-tuple-element.13.wb_ref, f32[10,16,128]{2,1,0:T(8,128)S(1)} %get-tuple-element.14.tab_ref), custom_call_target="tpu_custom_call" | custom-call | tf_op jit(solution)/shard_map/ends/pallas_call | solution.py:318
  13.1 6.4 %all-to-all-start.1 = ((f32[8,32,128]{2,1,0:T(8,128)}), f32[8,32,128]{2,1,0:T(8,128)S(1)}, u32[]{:S(2)}, u32[]{:S(2)}) async-start(f32[8,32,128]{2,1,0:T(8,128)} %get-tuple-element.15), calls=%async_computation.1 | async-start | bytes 262144 | tf_op jit(solution)/shard_map/all_to_all | solution.py:333
  19.5 3.8 %local.1 = (f32[192,512]{1,0:T(8,128)}, bf16[4,128,1024]{2,1,0:T(8,128)(2,1)S(1)}, f32[10,16,128]{2,1,0:T(8,128)S(1)}) custom-call(bf16[192,512]{1,0:T(8,128)(2,1)} %get-tuple-element.16.up_hbm, f32[2,16,8,128]{3,2,1,0:T(8,128)} %get-tuple-element.17.init_hbm, f32[512,64]{1,0:T(8,128)} %bitcast.18, f32[512,64]{1,0:T(8,128)} %bitcast.20, f32[512,64]{1,0:T(8,128)} %bitcast.21, ...), custom_call_target="tpu_custom_call" | custom-call | tf_op jit(solution)/shard_map/local/pallas_call | solution.py:334
  23.3 3.5 %all-to-all-done.1.end_ref = f32[8,32,128]{2,1,0:T(8,128)S(1)} async-done(((f32[8,32,128]{2,1,0:T(8,128)}), f32[8,32,128]{2,1,0:T(8,128)S(1)}, u32[]{:S(2)}, u32[]{:S(2)}) %all-to-all-start.1) | async-done | bytes 131104 | tf_op jit(solution)/shard_map/all_to_all | solution.py:333
  26.9 0.0 copy-start.1
  26.9 2.3 %carry.1 = bf16[192,512]{1,0:T(8,128)(2,1)S(1)} custom-call(s32[1]{0:T(128)} %bitcast.mine_ref, f32[8,32,128]{2,1,0:T(8,128)S(1)} %all-to-all-done.1.end_ref, f32[192,512]{1,0:T(8,128)} %get-tuple-element.18.y_hbm, bf16[4,128,1024]{2,1,0:T(8,128)(2,1)S(1)} %get-tuple-element.19.cw_ref, f32[10,16,128]{2,1,0:T(8,128)S(1)} %get-tuple-element.20.tab_ref), custom_call_target="tpu_custom_call" | custom-call | tf_op jit(solution)/shard_map/carry/pallas_call | solution.py:370
  29.2 7.5 %all_gather.3 = bf16[192,2048]{1,0:T(8,128)(2,1)S(1)} all-gather(bf16[192,512]{1,0:T(8,128)(2,1)S(1)} %carry.1), channel_id=1, replica_groups=mesh['sp'=8,'tp'=4] {'tp'}, dimensions={1}, use_global_device_ids=true | all-gather | bytes 983040 | tf_op jit(solution)/shard_map/all_gather | solution.py:383
  36.7 0.0 copy-done.1
  36.7 0.6 %fusion.4 = f32[192,512]{1,0:T(8,128)S(1)} fusion(bf16[192,2048]{1,0:T(8,128)(2,1)S(1)} %all_gather.3, bf16[2048,512]{1,0:T(8,128)(2,1)S(1)} %copy-done.1), kind=kOutput, calls=%fused_computation.8 | convolution fusion | flops 402653184 | bytes 3276800 | tf_op jit(solution)/shard_map/dot_general | solution.py:384
  37.2 0.0 copy-done
  37.3 0.0 copy-start.2
  37.3 0.7 %multiply_reduce_fusion = (f32[192]{0:T(256)S(1)}, f32[192,512]{1,0:T(8,128)S(1)}) fusion(f32[192,512]{1,0:T(8,128)S(1)} %fusion.4, bf16[192,2048]{1,0:T(8,128)(2,1)S(1)} %all_gather.3, bf16[2048,512]{1,0:T(8,128)(2,1)S(1)} %copy-done), kind=kOutput, calls=%fused_computation.6 | convolution fusion | flops 403242816 | bytes 3670784 | tf_op jit(solution)/shard_map/dot_general | solution.py:385
  38.0 7.2 %psum.7 = f32[192]{0:T(256)S(1)} all-reduce(f32[192]{0:T(256)S(1)} %get-tuple-element.21), channel_id=1, replica_groups=mesh['sp'=8,'tp'=4] {'tp'}, use_global_device_ids=true, to_apply=%region_1.0 | all-reduce | flops 192 | bytes 1536 | tf_op jit(solution)/shard_map/psum | solution.py:387
  45.3 0.0 copy-done.2
  45.3 0.8 %multiply_convert_fusion = bf16[192,512]{1,0:T(8,128)(2,1)} fusion(f32[192,512]{1,0:T(8,128)S(1)} %get-tuple-element.22, f32[512]{0:T(512)S(1)} %copy-done.2, f32[192]{0:T(256)S(1)} %add_rsqrt_fusion), kind=kLoop, calls=%fused_computation.5 | loop fusion | flops 294912 | bytes 592640 | tf_op jit(solution)/shard_map/convert_element_type | solution.py:389
  (1 shorter events, 0.0 us)
Async XLA Ops:
  0.0 37.2 %copy-start = (bf16[2048,512]{1,0:T(8,128)(2,1)S(1)}, bf16[2048,512]{1,0:T(8,128)(2,1)}, u32[]{:S(2)}) copy-start(bf16[2048,512]{1,0:T(8,128)(2,1)} %param.22) | copy-start | bytes 6291460
  1.9 9.5 %all-to-all-start = ((bf16[4,48,512]{2,1,0:T(8,128)(2,1)}), bf16[4,48,512]{2,1,0:T(8,128)(2,1)S(1)}, u32[]{:S(2)}, u32[]{:S(2)}) async-start(bf16[4,48,512]{2,1,0:T(8,128)(2,1)} %norm.1), calls=%async_computation | async-start | bytes 393216 | tf_op jit(solution)/shard_map/all_to_all | solution.py:308
  13.1 13.8 %all-to-all-start.1 = ((f32[8,32,128]{2,1,0:T(8,128)}), f32[8,32,128]{2,1,0:T(8,128)S(1)}, u32[]{:S(2)}, u32[]{:S(2)}) async-start(f32[8,32,128]{2,1,0:T(8,128)} %get-tuple-element.15), calls=%async_computation.1 | async-start | bytes 262144 | tf_op jit(solution)/shard_map/all_to_all | solution.py:333
  26.9 9.8 %copy-start.1 = (bf16[2048,512]{1,0:T(8,128)(2,1)S(1)}, bf16[2048,512]{1,0:T(8,128)(2,1)}, u32[]{:S(2)}) copy-start(bf16[2048,512]{1,0:T(8,128)(2,1)} %param.21) | copy-start | bytes 6291460
  37.3 8.0 %copy-start.2 = (f32[512]{0:T(512)S(1)}, f32[512]{0:T(512)}, u32[]{:S(2)}) copy-start(f32[512]{0:T(512)} %param.23) | copy-start | bytes 6148
